TPU v7x, 32 devices: a whole 2x2x4 slice. The times are simulated.
32 devices in a mesh: dp: 4 (over y, x), kv: 4 (over z), tp: 2 (over core).
Axes of the slice: x: 2, y: 2, z: 4, core: 2. Of those that a mesh axis runs over, the one named last changes fastest.
Arguments:
- tokens: bfloat16 [64, 16, 2048], P('dp'), may hold values from -6 to 6
- norm_gain: float32 [2048], replicated, may hold values from 0.1 to 1.9
- query_weight: bfloat16 [2048, 1024], P(None, 'tp'), may hold values from -0.125 to 0.125
- key_weight: bfloat16 [2048, 256], P(None, 'tp'), may hold values from -0.125 to 0.125
- value_weight: bfloat16 [2048, 256], P(None, 'tp'), may hold values from -0.125 to 0.125
- forget_weight: bfloat16 [2048, 8], replicated, may hold values from -0.125 to 0.125
- forget_bias: float32 [8], replicated, may hold values from 0 to 4
- query_gain: float32 [128], replicated, may hold values from 0.1 to 1.9
- key_gain: float32 [128], replicated, may hold values from 0.1 to 1.9
- output_weight: bfloat16 [1024, 2048], P('tp', 'kv'), may hold values from -0.1875 to 0.1875
- cache_keys: bfloat16 [64, 1024, 2, 128], P('dp', 'kv', 'tp'), may hold values from -512 to 512
- cache_values: bfloat16 [64, 1024, 2, 128], P('dp', 'kv', 'tp'), may hold values from -6 to 6
- cache_logcum: float32 [64, 1024, 8], P('dp', 'kv', 'tp'), may hold values from -205 to 0, as said below
- pending_keys: bfloat16 [64, 4, 2, 128], P('dp', None, 'tp'), may hold values from -6 to 6
- pending_values: bfloat16 [64, 4, 2, 128], P('dp', None, 'tp'), may hold values from -6 to 6
- pending_logcum: float32 [64, 4, 8], P('dp', None, 'tp'), may hold values from -205 to 0, as said below
- lengths: int32 [64], P('dp'), may hold values from 512 to 1020, as said below
- accepted: int32 [64], P('dp'), may hold values from 1 to 4
- parents: int32 [64, 16], P('dp'), may hold values from -1 to 14, as said below
Outputs:
- result: bfloat16 [64, 16, 2048], P('dp', None, ('kv', 'tp'))
Inputs may be any that keep to these rules, and one draw needn't show every extreme that they name: Positions below lengths hold a sequence's past; the last step's accepted proposals go to positions lengths to lengths + accepted - 1. `parents`: the parent of proposal i is -1 (the last accepted token) or a proposal before i. `cache_logcum`: non-increasing along positions for every sequence and head. `pending_logcum`: the cumulative log gates at positions lengths to lengths + 3, continuing cache_logcum.
All inputs are finite; a program needn't handle non-finite values.
Results may differ from a plain program's by a relative error of at most 0.014.
Values may be sent and summed in bfloat16 or wider, within the bound.
A program may use at most 128 MiB of HBM per device.

v0:
```python
import functools

import jax
import jax.numpy as jnp
from jax import lax
from jax.experimental import pallas as pl
from jax.experimental.pallas import tpu as pltpu
from jax.sharding import PartitionSpec as P

EPSILON = 1e-06
NEG_LARGE = -1e30
HIGHEST = lax.Precision.HIGHEST


def joined(shard, axis, join):
    gathered = jax.tree.map(
        lambda a, kind: lax.all_gather(a.astype(kind), axis),
        shard,
        (jnp.bfloat16, jnp.bfloat16, jnp.bfloat16),
    )

    def take(source):
        return jax.tree.map(
            lambda a, own: lax.dynamic_index_in_dim(a, source, 0, False).astype(own.dtype),
            gathered,
            shard,
        )

    return lax.fori_loop(
        1, lax.axis_size(axis), lambda source, state: join(state, take(source)), take(0)
    )


def head_norm(vectors, gain_vec):
    return (
        vectors
        * lax.rsqrt(jnp.mean(vectors * vectors, axis=-1, keepdims=True) + EPSILON)
        * gain_vec
    )


def ancestors(parents):
    node_count = parents.shape[-1]
    indices = jnp.arange(node_count, dtype=jnp.int32)
    reachable = (parents[..., None] == indices).astype(jnp.float32) + jnp.eye(
        node_count, dtype=jnp.float32
    )
    for doubling in range((node_count - 1).bit_length()):
        reachable = jnp.minimum(
            jnp.einsum("sij,sjk->sik", reachable, reachable, precision=HIGHEST), 1.0
        )
    return reachable


def join_blocks(earlier, later):
    larger = jnp.maximum(earlier[0], later[0])
    left_factor = jnp.exp(earlier[0] - larger)
    right_factor = jnp.exp(later[0] - larger)
    return (
        larger,
        earlier[1] * left_factor + later[1] * right_factor,
        earlier[2] * left_factor[..., None] + later[2] * right_factor[..., None],
    )


def to_rows(values):
    moved = jnp.swapaxes(values, 1, 2)
    return moved.reshape((moved.shape[0] * moved.shape[1],) + moved.shape[2:])


def finish_rows(cache_max, cache_sum, cache_acc, tree_max, tree_sum, tree_acc):
    overall = jnp.maximum(cache_max, tree_max)
    factor_cache = jnp.exp(cache_max - overall)
    factor_tree = jnp.exp(tree_max - overall)
    denominator = cache_sum * factor_cache + tree_sum * factor_tree
    numerator = cache_acc * factor_cache[..., None] + tree_acc * factor_tree[..., None]
    attended = (numerator / denominator[..., None]).astype(jnp.bfloat16)
    return attended.reshape(attended.shape[0], attended.shape[1] * attended.shape[2])


def shards(
    tokens,
    norm_gain,
    query_weight,
    key_weight,
    value_weight,
    forget_weight,
    forget_bias,
    query_gain,
    key_gain,
    output_weight,
    cache_keys,
    cache_values,
    cache_logcum,
    pending_keys,
    pending_values,
    pending_logcum,
    lengths,
    accepted,
    parents,
):
    seq_count, node_count, model_width = tokens.shape
    token_rows = seq_count * node_count
    head_size = query_gain.shape[0]
    query_cols = query_weight.shape[1]
    key_cols = key_weight.shape[1]
    local_heads = query_cols // head_size
    key_heads = key_cols // head_size
    sharing = local_heads // key_heads
    block_len = cache_keys.shape[1]
    most_taken = pending_keys.shape[1]
    scaling = head_size ** (-0.5)
    widened = tokens.reshape(token_rows, model_width).astype(jnp.float32)
    normed = (
        widened
        * lax.rsqrt(jnp.mean(widened * widened, axis=-1, keepdims=True) + EPSILON)
        * norm_gain
    ).astype(jnp.bfloat16)
    joined_weight = jnp.concatenate([query_weight, key_weight, value_weight], axis=1)
    summed = jnp.dot(normed, joined_weight, preferred_element_type=jnp.float32)
    query_part = head_norm(
        summed[:, :query_cols].reshape(token_rows, local_heads, head_size), query_gain
    )
    key_part = head_norm(
        summed[:, query_cols : query_cols + key_cols].reshape(token_rows, key_heads, head_size),
        key_gain,
    )
    queries = query_part.astype(jnp.bfloat16).reshape(
        seq_count, node_count, key_heads, sharing, head_size
    )
    keys_new = key_part.astype(jnp.bfloat16).reshape(seq_count, node_count, key_heads, head_size)
    values_new = (
        summed[:, query_cols + key_cols :]
        .astype(jnp.bfloat16)
        .reshape(seq_count, node_count, key_heads, head_size)
    )
    head_start = lax.axis_index("tp") * local_heads
    forget_cols = lax.dynamic_slice_in_dim(forget_weight, head_start, local_heads, 1)
    gate_bias = lax.dynamic_slice_in_dim(forget_bias, head_start, local_heads, 0)
    log_gates = jax.nn.log_sigmoid(
        jnp.dot(normed, forget_cols, preferred_element_type=jnp.float32) + gate_bias
    ).reshape(seq_count, node_count, local_heads)
    ancestry = ancestors(parents)
    choose = (jnp.arange(most_taken, dtype=jnp.int32)[None, :] == (accepted - 1)[:, None]).astype(
        jnp.float32
    )
    base_gate = jnp.einsum("sa,sah->sh", choose, pending_logcum, precision=HIGHEST)
    cumulative = base_gate[:, None, :] + jnp.einsum(
        "sij,sjh->sih", ancestry, log_gates, precision=HIGHEST
    )
    gate_rows = jnp.swapaxes(cumulative, 1, 2)
    token_place = lax.axis_index("kv") * block_len + jnp.arange(block_len, dtype=jnp.int32)
    offset = token_place[None, :] - lengths[:, None]
    inserted = (offset >= 0) & (offset < accepted[:, None])
    one_hot = (offset[..., None] == jnp.arange(most_taken, dtype=jnp.int32)) & inserted[..., None]
    hot_low = one_hot.astype(jnp.bfloat16)
    merged_keys = jnp.where(
        inserted[..., None, None],
        jnp.einsum(
            "sla,sakd->slkd", hot_low, pending_keys, preferred_element_type=jnp.float32
        ).astype(jnp.bfloat16),
        cache_keys,
    )
    merged_values = jnp.where(
        inserted[..., None, None],
        jnp.einsum(
            "sla,sakd->slkd", hot_low, pending_values, preferred_element_type=jnp.float32
        ).astype(jnp.bfloat16),
        cache_values,
    )
    log_cache = jnp.where(
        inserted[..., None],
        jnp.einsum("sla,sah->slh", one_hot.astype(jnp.float32), pending_logcum, precision=HIGHEST),
        cache_logcum,
    )
    usable = token_place[None, :] < (lengths + accepted)[:, None]
    raw_scores = jnp.einsum(
        "spkgd,slkd->skgpl", queries, merged_keys, preferred_element_type=jnp.float32
    )
    scores = (
        raw_scores.reshape(seq_count, local_heads, node_count, block_len) * scaling
        + gate_rows[..., None]
        - jnp.swapaxes(log_cache, 1, 2)[:, :, None, :]
    )
    visible = usable[:, None, None, :]
    block_max = jnp.max(jnp.where(visible, scores, NEG_LARGE), axis=-1)
    weights = jnp.where(visible, jnp.exp(scores - block_max[..., None]), 0.0)
    block_sum = jnp.sum(weights, axis=-1)
    block_acc = jnp.einsum(
        "skgpl,slkd->skgpd",
        weights.astype(jnp.bfloat16).reshape(seq_count, key_heads, sharing, node_count, block_len),
        merged_values,
        preferred_element_type=jnp.float32,
    )
    block_acc = block_acc.reshape(seq_count, local_heads, node_count, head_size)
    tree_raw = jnp.einsum(
        "spkgd,sjkd->skgpj", queries, keys_new, preferred_element_type=jnp.float32
    )
    tree_scores = (
        tree_raw.reshape(seq_count, local_heads, node_count, node_count) * scaling
        + gate_rows[..., :, None]
        - gate_rows[..., None, :]
    )
    tree_mask = ancestry[:, None] > 0.5
    tree_max = jnp.max(jnp.where(tree_mask, tree_scores, NEG_LARGE), axis=-1)
    tree_weights = jnp.where(tree_mask, jnp.exp(tree_scores - tree_max[..., None]), 0.0)
    tree_sum = jnp.sum(tree_weights, axis=-1)
    tree_acc = jnp.einsum(
        "skgpj,sjkd->skgpd",
        tree_weights.astype(jnp.bfloat16).reshape(
            seq_count, key_heads, sharing, node_count, node_count
        ),
        values_new,
        preferred_element_type=jnp.float32,
    )
    tree_acc = tree_acc.reshape(seq_count, local_heads, node_count, head_size)
    tree_max_rows = to_rows(tree_max)
    tree_sum_rows = to_rows(tree_sum)
    tree_acc_rows = to_rows(tree_acc)
    cache_max, cache_sum, cache_acc = joined((block_max, block_sum, block_acc), "kv", join_blocks)
    attended = finish_rows(
        to_rows(cache_max),
        to_rows(cache_sum),
        to_rows(cache_acc),
        tree_max_rows,
        tree_sum_rows,
        tree_acc_rows,
    )
    head_part = jnp.dot(attended, output_weight, preferred_element_type=jnp.float32)
    head_part = head_part.reshape(seq_count, node_count, output_weight.shape[1])
    return lax.psum_scatter(head_part.astype(jnp.bfloat16), "tp", scatter_dimension=2, tiled=True)


LANES = 128
STAT_ROWS = 8
VMEM_LIMIT = 60 * 1024 * 1024
LARGE = 1e30
LOG2_E = 1.4426950408889634
TOKEN_PIECES = 4


def contract_last(left, right):
    return lax.dot_general(
        left, right, (((1,), (1,)), ((), ())), preferred_element_type=jnp.float32
    )


def plain_dot(left, right):
    return jnp.dot(left, right, preferred_element_type=jnp.float32)


def fused_kernel(ring, pair, pieces, names, order, *refs):
    inputs = dict(zip(names, refs))
    out_ref = refs[len(names)]
    held = dict(zip(names, refs[len(names) + 1 :]))
    (
        weight_buf,
        normed_buf,
        query_buf,
        part_buf,
        part_recv,
        stat_buf,
        stat_recv,
        att_buf,
        half_send,
        half_mine,
        half_recv,
        load_sem,
        token_sem,
        part_send_sem,
        part_recv_sem,
        stat_send_sem,
        stat_recv_sem,
        att_send_sem,
        att_recv_sem,
        half_send_sem,
        half_recv_sem,
    ) = refs[2 * len(names) + 1 - 3 :]
    me = lax.axis_index("kv")
    core = lax.axis_index("tp")
    partner = 1 - core
    tokens_buf, keys_buf, values_buf = held["tokens"], held["cache_keys"], held["cache_values"]
    seqs, heads, nodes, head_size = query_buf.shape
    rows, width = tokens_buf.shape
    block_len = keys_buf.shape[1]
    most_taken = held["pend_log"].shape[0]
    pend_rows = held["pend_keys"].shape[0]
    chunk = seqs // ring
    own_rows = chunk * nodes
    seq_rows = heads * nodes
    query_cols = heads * head_size
    half_cols = half_send.shape[2]
    seqs_per_tile = LANES // seq_rows
    tiles = chunk // seqs_per_tile
    tile_rows = seqs_per_tile * nodes
    scaling = head_size ** (-0.5)
    exponent = scaling * LOG2_E

    def target(step):
        low = jnp.where(ring - 1 - step > me, ring - 1 - step, ring - 2 - step)
        high = jnp.where(step < me, step, step + 1)
        return jnp.where(me < ring // 2, low, high)

    barrier = pltpu.get_barrier_semaphore()
    for step in range(ring - 1):
        pl.semaphore_signal(barrier, inc=1, device_id={"kv": lax.rem(me + step + 1, ring)})
    pl.semaphore_signal(barrier, inc=1, device_id={"tp": partner})

    places = dict(held)
    places["query_weight"] = weight_buf.at[:, 0:query_cols]
    places["key_weight"] = weight_buf.at[:, query_cols : query_cols + head_size]
    places["value_weight"] = weight_buf.at[:, query_cols + head_size : query_cols + 2 * head_size]
    piece_rows = rows // pieces
    token_loads = []
    for piece in range(pieces):
        span = pl.ds(piece * piece_rows, piece_rows)
        token_loads.append(
            pltpu.make_async_copy(
                inputs["tokens"].at[span], tokens_buf.at[span], token_sem.at[piece]
            )
        )
    loads = {
        name: pltpu.make_async_copy(inputs[name], places[name], load_sem.at[number])
        for number, name in enumerate(names)
        if name != "tokens"
    }
    loads["norm_gain"].start()
    for load in token_loads:
        load.start()
    loads["query_weight"].start()

    loads["norm_gain"].wait()
    gain = held["norm_gain"][...]
    step_rows = 16
    for piece in range(pieces):
        token_loads[piece].wait()
        if piece == 0:
            for name in order:
                if name not in ("tokens", "norm_gain", "query_weight"):
                    loads[name].start()

        def norm_rows(index, carry):
            place = pl.multiple_of(piece * piece_rows + index * step_rows, step_rows)
            span = pl.ds(place, step_rows)
            wide = tokens_buf[span, :].astype(jnp.float32)
            mean = jnp.sum(wide * wide, axis=-1, keepdims=True) * (1.0 / width)
            normed_buf[span, :] = (wide * lax.rsqrt(mean + EPSILON) * gain).astype(jnp.bfloat16)
            return carry

        lax.fori_loop(0, piece_rows // step_rows, norm_rows, 0, unroll=4)

    def head_scaled(vectors, gain_vec):
        mean = jnp.sum(vectors * vectors, axis=-1, keepdims=True) * (1.0 / head_size)
        return (vectors * lax.rsqrt(mean + EPSILON) * gain_vec).astype(jnp.bfloat16)

    loads["query_weight"].wait()
    loads["query_gain"].wait()
    for start in range(0, query_cols, 2 * head_size):
        part = plain_dot(normed_buf[...], weight_buf[:, start : start + 2 * head_size])
        for inner in range(2):
            vectors = part[:, inner * head_size : (inner + 1) * head_size]
            query_buf[:, start // head_size + inner] = head_scaled(
                vectors, held["query_gain"][...]
            ).reshape(seqs, nodes, head_size)

    for name in ("lengths", "cache_log", "cache_keys", "cache_values"):
        loads[name].wait()

    place = me * block_len + lax.broadcasted_iota(jnp.int32, (heads, block_len), 1)
    diagonal = lax.broadcasted_iota(jnp.int32, (LANES, LANES), 0) == lax.broadcasted_iota(
        jnp.int32, (LANES, LANES), 1
    )
    ones = jnp.ones((block_len, head_size), jnp.bfloat16)

    def spread_heads(table):
        return jnp.concatenate(
            [
                jnp.broadcast_to(table[head : head + 1, :], (nodes, table.shape[1]))
                for head in range(heads)
            ],
            axis=0,
        )

    def soft_part(scores, values, units):
        top = jnp.max(scores, axis=-1, keepdims=True)
        weights = jnp.exp2((scores - top) * exponent).astype(jnp.bfloat16)
        both = plain_dot(weights, jnp.concatenate([values, units], axis=1))
        total = both[:, head_size:]
        return both[:, :head_size] / total, top * scaling + jnp.log(total)

    def row_form(stats):
        column = jnp.concatenate(stats, axis=0)
        return jnp.sum(jnp.where(diagonal, column, 0.0), axis=0, keepdims=True)

    def stat_rows(stats):
        found = [
            row_form(stats[tile * seqs_per_tile : (tile + 1) * seqs_per_tile])
            for tile in range(tiles)
        ]
        return jnp.concatenate(
            found + [jnp.zeros((STAT_ROWS - tiles, LANES), jnp.float32)], axis=0
        )

    def attend(owner):
        values, stats = [], []
        for inner in range(chunk):
            seq = owner * chunk + inner
            query = query_buf[seq].reshape(seq_rows, head_size)
            bias = jnp.where(
                place < held["lengths"][seq], held["cache_log"][seq] * (1.0 / scaling), LARGE
            )
            scores = contract_last(query, keys_buf[seq]) - spread_heads(bias)
            value, stat = soft_part(scores, values_buf[seq], ones)
            values.append(value)
            stats.append(stat)
        return values, stats

    def send_part(step):
        there = target(step)
        return (
            pltpu.make_async_remote_copy(
                part_buf.at[step],
                part_recv.at[me],
                part_send_sem.at[step],
                part_recv_sem.at[me],
                device_id={"kv": there},
            ),
            pltpu.make_async_remote_copy(
                stat_buf.at[step],
                stat_recv.at[me],
                stat_send_sem.at[step],
                stat_recv_sem.at[me],
                device_id={"kv": there},
            ),
        )

    sends = []
    for step in range(ring - 1):
        values, stats = attend(target(step))
        for inner in range(chunk):
            part_buf[step, inner * seq_rows : (inner + 1) * seq_rows, :] = values[inner].astype(
                jnp.bfloat16
            )
        stat_buf[step] = stat_rows(stats)
        if step == 0:
            pl.semaphore_wait(barrier, ring)
        for copy in send_part(step):
            copy.start()
            sends.append(copy)

    own_values, own_stats = attend(me)
    own_stats = stat_rows(own_stats)

    for name in ("parents", "forget", "forget_bias", "accepted", "pend_log"):
        loads[name].wait()
    row_id = lax.broadcasted_iota(jnp.int32, (own_rows, seqs), 0)
    lane_id = lax.broadcasted_iota(jnp.int32, (own_rows, seqs), 1)
    spread = jnp.where(row_id // nodes + me * chunk == lane_id, 1.0, 0.0).astype(jnp.bfloat16)
    parent_rows = plain_dot(spread, held["parents"][...].astype(jnp.float32).astype(jnp.bfloat16))
    node_row = lax.broadcasted_iota(jnp.int32, (own_rows, nodes), 0)
    node_lane = lax.broadcasted_iota(jnp.int32, (own_rows, nodes), 1)
    parent = jnp.sum(
        jnp.where(node_row % nodes == node_lane, parent_rows, 0.0), axis=-1, keepdims=True
    )
    wide_row = lax.broadcasted_iota(jnp.int32, (own_rows, own_rows), 0)
    wide_lane = lax.broadcasted_iota(jnp.int32, (own_rows, own_rows), 1)
    lane_in_seq = (wide_lane - (wide_row // nodes) * nodes).astype(jnp.float32)
    linked = ((lane_in_seq == parent) & (parent >= 0.0)) | (wide_row == wide_lane)
    reach = jnp.where(linked, 1.0, 0.0).astype(jnp.bfloat16)
    for doubling in range((nodes - 1).bit_length()):
        reach = jnp.minimum(plain_dot(reach, reach), 1.0).astype(jnp.bfloat16)

    mine = pl.ds(pl.multiple_of(me * own_rows, own_rows), own_rows)
    own_normed = normed_buf[mine, :]
    all_heads = held["forget"].shape[0]
    square = (all_heads, all_heads)
    bias_column = jnp.sum(
        jnp.where(
            lax.broadcasted_iota(jnp.int32, square, 0) == lax.broadcasted_iota(jnp.int32, square, 1),
            jnp.broadcast_to(held["forget_bias"][...], square),
            0.0,
        ),
        axis=-1,
        keepdims=True,
    )
    logits = contract_last(held["forget"][...], own_normed) + bias_column
    log_gates = jnp.minimum(logits, 0.0) - jnp.log1p(jnp.exp(-jnp.abs(logits)))
    high = log_gates.astype(jnp.bfloat16)
    rest = log_gates - high.astype(jnp.float32)
    middle = rest.astype(jnp.bfloat16)
    low = (rest - middle.astype(jnp.float32)).astype(jnp.bfloat16)
    summed = contract_last(high, reach) + contract_last(middle, reach) + contract_last(low, reach)
    gates = summed[0:heads]
    for other in range(1, pair):
        gates = jnp.where(core == other, summed[other * heads : (other + 1) * heads], gates)

    for name in ("key_weight", "value_weight", "key_gain", "pend_keys", "pend_values"):
        loads[name].wait()
    part = plain_dot(own_normed, weight_buf[:, query_cols : query_cols + 2 * head_size])
    tree_keys = jnp.concatenate(
        [head_scaled(part[:, :head_size], held["key_gain"][...]), held["pend_keys"][...]], axis=0
    )
    tree_values = jnp.concatenate(
        [part[:, head_size:].astype(jnp.bfloat16), held["pend_values"][...]], axis=0
    )

    gate_head = lax.broadcasted_iota(jnp.int32, (heads, own_rows), 0)
    gate_seq = lax.broadcasted_iota(jnp.int32, (heads, own_rows), 1) // nodes
    pend_head = lax.broadcasted_iota(jnp.int32, (heads, pend_rows), 0)
    pend_lane = lax.broadcasted_iota(jnp.int32, (heads, pend_rows), 1)
    pend_bias = jnp.zeros((heads, pend_rows), jnp.float32)
    pend_seen = []
    pend_place = lax.broadcasted_iota(jnp.int32, (seq_rows, pend_rows), 1)
    for inner in range(chunk):
        seq = me * chunk + inner
        took = held["accepted"][seq]
        last_taken = jnp.maximum(took - 1, 0)
        first = seq * most_taken
        pend_seen.append((pend_place >= first) & (pend_place < first + took))
        for head in range(heads):
            base = held["pend_log"][last_taken, head, seq]
            gates = jnp.where((gate_head == head) & (gate_seq == inner), gates + base, gates)
            for number in range(most_taken):
                pend_bias = jnp.where(
                    (pend_head == head) & (pend_lane == first + number),
                    held["pend_log"][number, head, seq],
                    pend_bias,
                )
    tree_bias = spread_heads(
        jnp.concatenate([gates, pend_bias], axis=1) * (1.0 / scaling)
    )
    gate_stats = jnp.concatenate(
        [
            jnp.concatenate(
                [
                    gates[head : head + 1, inner * nodes : (inner + 1) * nodes]
                    for inner in range(tile * seqs_per_tile, (tile + 1) * seqs_per_tile)
                    for head in range(heads)
                ],
                axis=1,
            )
            for tile in range(tiles)
        ]
        + [jnp.zeros((STAT_ROWS - tiles, LANES), jnp.float32)],
        axis=0,
    )
    reached = reach.astype(jnp.float32)
    tree_ones = jnp.ones((own_rows + pend_rows, head_size), jnp.bfloat16)
    tree_parts, tree_stats = [], []
    for inner in range(chunk):
        query = query_buf[me * chunk + inner].reshape(seq_rows, head_size)
        seen = jnp.concatenate(
            [
                jnp.concatenate([reached[inner * nodes : (inner + 1) * nodes, :]] * heads, axis=0),
                jnp.where(pend_seen[inner], 1.0, 0.0),
            ],
            axis=1,
        )
        scores = contract_last(query, tree_keys) - jnp.where(seen > 0.5, tree_bias, LARGE)
        value, stat = soft_part(scores, tree_values, tree_ones)
        tree_parts.append(value)
        tree_stats.append(stat)
    tree_stats = stat_rows(tree_stats)

    for step in range(ring - 1):
        source = target(step)
        for buffer, received, send_sems, recv_sems in (
            (part_buf, part_recv, part_send_sem, part_recv_sem),
            (stat_buf, stat_recv, stat_send_sem, stat_recv_sem),
        ):
            pltpu.make_async_remote_copy(
                buffer.at[step],
                received.at[source],
                send_sems.at[step],
                recv_sems.at[source],
                device_id={"kv": source},
            ).wait_recv()
    stats = [tree_stats, own_stats] + [
        stat_recv[target(step)] for step in range(ring - 1)
    ]
    stats = [stat + gate_stats for stat in stats]
    top = functools.reduce(jnp.maximum, stats)
    factors = [jnp.exp(stat - top) for stat in stats]
    whole = functools.reduce(jnp.add, factors)
    factors = [factor / whole for factor in factors]
    blank = jnp.zeros((LANES - STAT_ROWS * len(factors), LANES), jnp.float32)
    factor_cols = jnp.concatenate(factors + [blank], axis=0).T
    for inner in range(chunk):
        tile = inner // seqs_per_tile
        lanes = slice((inner % seqs_per_tile) * seq_rows, (inner % seqs_per_tile + 1) * seq_rows)
        span = slice(inner * seq_rows, (inner + 1) * seq_rows)
        sources = [tree_parts[inner], own_values[inner]] + [
            part_recv[target(step), span, :].astype(jnp.float32) for step in range(ring - 1)
        ]
        mixed = None
        for number, source in enumerate(sources):
            lane = number * STAT_ROWS + tile
            term = factor_cols[lanes, lane : lane + 1] * source
            mixed = term if mixed is None else mixed + term
        mixed = mixed.astype(jnp.bfloat16)
        for head in range(heads):
            att_buf[
                me,
                inner * nodes : (inner + 1) * nodes,
                head * head_size : (head + 1) * head_size,
            ] = mixed[head * nodes : (head + 1) * nodes, :]
    att_sends = []
    for step in range(ring - 1):
        copy = pltpu.make_async_remote_copy(
            att_buf.at[me],
            att_buf.at[me],
            att_send_sem.at[step],
            att_recv_sem.at[me],
            device_id={"kv": target(step)},
        )
        copy.start()
        att_sends.append(copy)

    loads["output_weight"].wait()
    theirs = pl.ds(pl.multiple_of(partner * half_cols, LANES), half_cols)
    ours = pl.ds(pl.multiple_of(core * half_cols, LANES), half_cols)
    output_weight_buf = held["output_weight"]
    half_sends = []
    for spot in range(ring):
        origin = me if spot == 0 else target(ring - 1 - spot)
        if spot > 0:
            pltpu.make_async_remote_copy(
                att_buf.at[origin],
                att_buf.at[origin],
                att_send_sem.at[spot - 1],
                att_recv_sem.at[origin],
                device_id={"kv": origin},
            ).wait_recv()
        attended = att_buf[origin]
        half_send[spot] = plain_dot(attended, output_weight_buf[:, theirs]).astype(jnp.bfloat16)
        copy = pltpu.make_async_remote_copy(
            half_send.at[spot],
            half_recv.at[spot],
            half_send_sem.at[spot],
            half_recv_sem.at[spot],
            device_id={"tp": partner},
        )
        copy.start()
        half_sends.append(copy)
        half_mine[spot] = plain_dot(attended, output_weight_buf[:, ours]).astype(jnp.bfloat16)
    for spot in range(ring):
        origin = me if spot == 0 else target(ring - 1 - spot)
        half_sends[spot].wait_recv()
        out_ref[origin] = (
            half_mine[spot].astype(jnp.float32) + half_recv[spot].astype(jnp.float32)
        ).astype(jnp.bfloat16)
    for copy in sends + att_sends + half_sends:
        copy.wait_send()


def fused(
    ring,
    pair,
    tokens,
    norm_gain,
    query_weight,
    key_weight,
    value_weight,
    forget_weight,
    forget_bias,
    query_gain,
    key_gain,
    output_weight,
    cache_keys,
    cache_values,
    cache_logcum,
    pending_keys,
    pending_values,
    pending_logcum,
    lengths,
    accepted,
    parents,
):
    seqs, nodes, width = tokens.shape
    head_size = query_gain.shape[0]
    query_cols = query_weight.shape[1]
    heads = query_cols // head_size
    block_len = cache_keys.shape[1]
    rows = seqs * nodes
    half_cols = output_weight.shape[1] // pair
    chunk = seqs // ring
    chunk_rows = chunk * nodes
    part_rows = chunk_rows * heads
    pieces = TOKEN_PIECES if rows % (64 * TOKEN_PIECES) == 0 else 1
    arrays = {
        "tokens": tokens.reshape(rows, width),
        "norm_gain": norm_gain.reshape(1, width),
        "query_weight": query_weight,
        "query_gain": query_gain.reshape(1, head_size),
        "lengths": lengths,
        "cache_log": jnp.swapaxes(cache_logcum, 1, 2),
        "cache_keys": cache_keys.reshape(seqs, block_len, head_size),
        "cache_values": cache_values.reshape(seqs, block_len, head_size),
        "parents": parents,
        "forget": forget_weight.T,
        "forget_bias": forget_bias.reshape(1, -1),
        "accepted": accepted,
        "pend_log": jnp.transpose(pending_logcum, (1, 2, 0)),
        "key_weight": key_weight,
        "value_weight": value_weight,
        "key_gain": key_gain.reshape(1, head_size),
        "pend_keys": pending_keys.reshape(-1, head_size),
        "pend_values": pending_values.reshape(-1, head_size),
        "output_weight": output_weight,
    }
    scalars = ("lengths", "accepted", "pend_log")
    joined_loads = ("query_weight", "key_weight", "value_weight")
    names = tuple(name for name in arrays if name not in joined_loads) + joined_loads
    order = tuple(arrays)
    held = [
        (pltpu.SMEM if name in scalars else pltpu.VMEM)(arrays[name].shape, arrays[name].dtype)
        for name in names
        if name not in joined_loads
    ]
    low, wide = jnp.bfloat16, jnp.float32
    sems = pltpu.SemaphoreType.DMA
    result = pl.pallas_call(
        functools.partial(fused_kernel, ring, pair, pieces, names, order),
        out_shape=pltpu.VMEM((ring, chunk_rows, half_cols), low),
        in_specs=[pl.BlockSpec(memory_space=pltpu.HBM)] * len(names),
        out_specs=pl.BlockSpec(memory_space=pltpu.VMEM),
        scratch_shapes=held
        + [
            pltpu.VMEM((width, query_cols + 2 * head_size), low),
            pltpu.VMEM((rows, width), low),
            pltpu.VMEM((seqs, heads, nodes, head_size), low),
            pltpu.VMEM((ring - 1, part_rows, head_size), low),
            pltpu.VMEM((ring, part_rows, head_size), low),
            pltpu.VMEM((ring - 1, STAT_ROWS, LANES), wide),
            pltpu.VMEM((ring, STAT_ROWS, LANES), wide),
            pltpu.VMEM((ring, chunk_rows, query_cols), low),
            pltpu.VMEM((ring, chunk_rows, half_cols), low),
            pltpu.VMEM((ring, chunk_rows, half_cols), low),
            pltpu.VMEM((ring, chunk_rows, half_cols), low),
            sems((len(names),)),
            sems((pieces,)),
            sems((ring - 1,)),
            sems((ring,)),
            sems((ring - 1,)),
            sems((ring,)),
            sems((ring - 1,)),
            sems((ring,)),
            sems((ring,)),
            sems((ring,)),
        ],
        compiler_params=pltpu.CompilerParams(
            collective_id=0, has_side_effects=True, vmem_limit_bytes=VMEM_LIMIT
        ),
    )(*[arrays[name] for name in names])
    return result.reshape(seqs, nodes, half_cols)


def layer(ring, pair, *arrays):
    tokens, output_weight, cache_keys = arrays[0], arrays[9], arrays[10]
    seqs, nodes = tokens.shape[:2]
    head_size = arrays[7].shape[0]
    heads = arrays[2].shape[1] // head_size
    fits = (
        ring > 1
        and pair == 2
        and head_size == LANES
        and cache_keys.shape[2] == 1
        and cache_keys.shape[1] % LANES == 0
        and nodes % 16 == 0
        and LANES % (heads * nodes) == 0
        and heads % 2 == 0
        and seqs % ring == 0
        and (seqs // ring * heads * nodes) % LANES == 0
        and STAT_ROWS * (ring + 1) <= LANES
        and seqs // ring * heads * nodes // LANES <= STAT_ROWS
        and seqs // ring * nodes + seqs * arrays[13].shape[1] == LANES
        and (seqs * nodes) % LANES == 0
        and output_weight.shape[1] % (pair * LANES) == 0
    )
    if fits:
        return fused(ring, pair, *arrays)
    return shards(*arrays)


def solution(mesh):
    placed = (
        P("dp", None, None),
        P(),
        P(None, "tp"),
        P(None, "tp"),
        P(None, "tp"),
        P(),
        P(),
        P(),
        P(),
        P("tp", "kv"),
        P("dp", "kv", "tp", None),
        P("dp", "kv", "tp", None),
        P("dp", "kv", "tp"),
        P("dp", None, "tp", None),
        P("dp", None, "tp", None),
        P("dp", None, "tp"),
        P("dp"),
        P("dp"),
        P("dp", None),
    )
    return jax.shard_map(
        functools.partial(layer, mesh.shape["kv"], mesh.shape["tp"]), mesh=mesh, in_specs=placed, out_specs=P("dp", None, ("kv", "tp")), check_vma=False
    )
```

profile of v0, /device:TPU:0, one launch (start us, length us, event | category | flops | bytes accessed | tf_op | source)
XLA Modules:
  0.0 21.9 jit_solution(2878322841610160270)
XLA Ops:
  0.0 21.3 %shard_map.181 = bf16[4,64,256]{2,1,0:T(8,128)(2,1)S(1)} custom-call(bf16[256,2048]{1,0:T(8,128)(2,1)} %bitcast.14, f32[1,2048]{1,0:T(1,128)} %bitcast.21, f32[1,128]{1,0:T(1,128)} %bitcast.23, s32[16]{0:T(128)} %refs_3_.1, f32[16,4,256]{2,1,0:T(4,128)} %bitcast.17, bf16[16,256,128]{2,1,0:T(8,128)(2,1)} %bitcast.15, bf16[16,256,128]{2,1,0:T(8,128)(2,1)} %bitcast.16, ...), custom_call_target="tpu_custom_call" | custom-call | tf_op jit(solution)/shard_map/pallas_call | solution.py:722
  21.3 0.7 %copy.21 = bf16[16,16,256]{2,1,0:T(8,128)(2,1)} copy(bf16[16,16,256]{2,1,0:T(8,128)(2,1)S(1)} %bitcast.13) | data formatting | bytes 262144
where the time goes:
time: 22.1 us; the launch traced here: 21.9 us
  Pallas kernels  21.3 us (96%)
  local copies, waits for them, and re-layouts  0.66 us (3%)
    pallas_call x1, Pallas kernels, fused(): pl.pallas_call(functools.partial(fused_kernel, ring, pair, pieces, names,...  21.3 us
    unnamed x1, local copies, waits for them, and re-layouts  0.66 us

commit v1 on v0

--- a/solution.py
+++ b/solution.py
@@ -233,6 +233,7 @@
 
 LANES = 128
 STAT_ROWS = 8
+STAT_PARTS = 3
 VMEM_LIMIT = 60 * 1024 * 1024
 LARGE = 1e30
 LOG2_E = 1.4426950408889634
@@ -259,26 +260,25 @@
         query_buf,
         part_buf,
         part_recv,
-        stat_buf,
-        stat_recv,
+        full_weight,
         att_buf,
         half_send,
-        half_mine,
         half_recv,
         load_sem,
         token_sem,
         part_send_sem,
         part_recv_sem,
-        stat_send_sem,
-        stat_recv_sem,
         att_send_sem,
         att_recv_sem,
         half_send_sem,
         half_recv_sem,
-    ) = refs[2 * len(names) + 1 - 3 :]
+        local_send_sem,
+        weight_sems,
+    ) = refs[2 * len(names) + 1 - 4 :]
     me = lax.axis_index("kv")
     core = lax.axis_index("tp")
     partner = 1 - core
+    last = pair - 1
     tokens_buf, keys_buf, values_buf = held["tokens"], held["cache_keys"], held["cache_values"]
     seqs, heads, nodes, head_size = query_buf.shape
     rows, width = tokens_buf.shape
@@ -293,21 +293,27 @@
     seqs_per_tile = LANES // seq_rows
     tiles = chunk // seqs_per_tile
     tile_rows = seqs_per_tile * nodes
+    part_rows = chunk * seq_rows
     scaling = head_size ** (-0.5)
     exponent = scaling * LOG2_E
 
     def target(step):
+        step = ring - 2 - step
         low = jnp.where(ring - 1 - step > me, ring - 1 - step, ring - 2 - step)
         high = jnp.where(step < me, step, step + 1)
         return jnp.where(me < ring // 2, low, high)
 
     barrier = pltpu.get_barrier_semaphore()
     for step in range(ring - 1):
-        pl.semaphore_signal(barrier, inc=1, device_id={"kv": lax.rem(me + step + 1, ring)})
+        for other in range(pair):
+            pl.semaphore_signal(
+                barrier, inc=1, device_id={"kv": lax.rem(me + step + 1, ring), "tp": other}
+            )
     pl.semaphore_signal(barrier, inc=1, device_id={"tp": partner})
 
     places = dict(held)
     places["query_weight"] = weight_buf.at[:, 0:query_cols]
+    places["output_weight"] = full_weight.at[core]
     places["key_weight"] = weight_buf.at[:, query_cols : query_cols + head_size]
     places["value_weight"] = weight_buf.at[:, query_cols + head_size : query_cols + 2 * head_size]
     piece_rows = rows // pieces
@@ -415,38 +421,54 @@
             stats.append(stat)
         return values, stats
 
-    def send_part(step):
-        there = target(step)
-        return (
-            pltpu.make_async_remote_copy(
-                part_buf.at[step],
-                part_recv.at[me],
-                part_send_sem.at[step],
-                part_recv_sem.at[me],
-                device_id={"kv": there},
-            ),
-            pltpu.make_async_remote_copy(
-                stat_buf.at[step],
-                stat_recv.at[me],
-                stat_send_sem.at[step],
-                stat_recv_sem.at[me],
-                device_id={"kv": there},
-            ),
+    def pack(stats):
+        rest = stats[0:tiles]
+        found = []
+        for number in range(STAT_PARTS):
+            found.append(rest.astype(jnp.bfloat16).astype(jnp.float32))
+            rest = rest - found[-1]
+        blank = jnp.zeros((2 * STAT_ROWS - STAT_PARTS * tiles, LANES), jnp.float32)
+        return jnp.concatenate(found + [blank], axis=0).astype(jnp.bfloat16)
+
+    def unpack(source):
+        packed = part_recv[source, part_rows : part_rows + 2 * STAT_ROWS, :].astype(jnp.float32)
+        return jnp.concatenate(
+            [
+                functools.reduce(
+                    jnp.add,
+                    [
+                        packed[number * tiles : (number + 1) * tiles]
+                        for number in range(STAT_PARTS)
+                    ],
+                ),
+                jnp.zeros((STAT_ROWS - tiles, LANES), jnp.float32),
+            ],
+            axis=0,
+        )
+
+    def send_part(step, there):
+        return pltpu.make_async_remote_copy(
+            part_buf.at[step],
+            part_recv.at[me],
+            part_send_sem.at[step],
+            part_recv_sem.at[me],
+            device_id={"kv": there},
         )
 
     sends = []
     for step in range(ring - 1):
-        values, stats = attend(target(step))
+        there = target(ring - 2 - step)
+        values, stats = attend(there)
         for inner in range(chunk):
             part_buf[step, inner * seq_rows : (inner + 1) * seq_rows, :] = values[inner].astype(
                 jnp.bfloat16
             )
-        stat_buf[step] = stat_rows(stats)
+        part_buf[step, part_rows : part_rows + 2 * STAT_ROWS, :] = pack(stat_rows(stats))
         if step == 0:
-            pl.semaphore_wait(barrier, ring)
-        for copy in send_part(step):
-            copy.start()
-            sends.append(copy)
+            pl.semaphore_wait(barrier, (ring - 1) * pair + 1)
+        copy = send_part(step, there)
+        copy.start()
+        sends.append(copy)
 
     own_values, own_stats = attend(me)
     own_stats = stat_rows(own_stats)
@@ -562,95 +584,140 @@
         tree_stats.append(stat)
     tree_stats = stat_rows(tree_stats)
 
-    for step in range(ring - 1):
-        source = target(step)
-        for buffer, received, send_sems, recv_sems in (
-            (part_buf, part_recv, part_send_sem, part_recv_sem),
-            (stat_buf, stat_recv, stat_send_sem, stat_recv_sem),
-        ):
-            pltpu.make_async_remote_copy(
-                buffer.at[step],
-                received.at[source],
-                send_sems.at[step],
-                recv_sems.at[source],
-                device_id={"kv": source},
-            ).wait_recv()
-    stats = [tree_stats, own_stats] + [
-        stat_recv[target(step)] for step in range(ring - 1)
-    ]
-    stats = [stat + gate_stats for stat in stats]
-    top = functools.reduce(jnp.maximum, stats)
-    factors = [jnp.exp(stat - top) for stat in stats]
-    whole = functools.reduce(jnp.add, factors)
-    factors = [factor / whole for factor in factors]
-    blank = jnp.zeros((LANES - STAT_ROWS * len(factors), LANES), jnp.float32)
-    factor_cols = jnp.concatenate(factors + [blank], axis=0).T
-    for inner in range(chunk):
+    def weigh(stats):
+        top = functools.reduce(jnp.maximum, stats)
+        factors = [jnp.exp(stat - top) for stat in stats]
+        whole = functools.reduce(jnp.add, factors)
+        factors = [factor / whole for factor in factors]
+        blank = jnp.zeros((LANES - STAT_ROWS * len(factors), LANES), jnp.float32)
+        return jnp.concatenate(factors + [blank], axis=0).T, top + jnp.log(whole)
+
+    def mix(columns, inner, sources):
         tile = inner // seqs_per_tile
-        lanes = slice((inner % seqs_per_tile) * seq_rows, (inner % seqs_per_tile + 1) * seq_rows)
-        span = slice(inner * seq_rows, (inner + 1) * seq_rows)
-        sources = [tree_parts[inner], own_values[inner]] + [
-            part_recv[target(step), span, :].astype(jnp.float32) for step in range(ring - 1)
-        ]
+        first = (inner % seqs_per_tile) * seq_rows
         mixed = None
         for number, source in enumerate(sources):
             lane = number * STAT_ROWS + tile
-            term = factor_cols[lanes, lane : lane + 1] * source
+            term = columns[first : first + seq_rows, lane : lane + 1] * source
             mixed = term if mixed is None else mixed + term
-        mixed = mixed.astype(jnp.bfloat16)
+        return mixed
+
+    columns, local_stats = weigh([tree_stats + gate_stats, own_stats + gate_stats])
+    local_parts = [
+        mix(columns, inner, [tree_parts[inner], own_values[inner]]) for inner in range(chunk)
+    ]
+
+    loads["output_weight"].wait()
+    weight_push = pltpu.make_async_remote_copy(
+        full_weight.at[0],
+        full_weight.at[0],
+        weight_sems.at[0],
+        weight_sems.at[1],
+        device_id={"tp": last},
+    )
+    pl.when(core != last)(weight_push.start)
+
+    for step in range(ring - 1):
+        source = target(step)
+        pltpu.make_async_remote_copy(
+            part_buf.at[step],
+            part_recv.at[source],
+            part_send_sem.at[step],
+            part_recv_sem.at[source],
+            device_id={"kv": source},
+        ).wait_recv()
+    columns, _ = weigh(
+        [local_stats] + [unpack(target(step)) + gate_stats for step in range(ring - 1)]
+    )
+    for inner in range(chunk):
+        span = slice(inner * seq_rows, (inner + 1) * seq_rows)
+        mixed = mix(
+            columns,
+            inner,
+            [local_parts[inner]]
+            + [part_recv[target(step), span, :].astype(jnp.float32) for step in range(ring - 1)],
+        ).astype(jnp.bfloat16)
         for head in range(heads):
             att_buf[
+                core,
                 me,
                 inner * nodes : (inner + 1) * nodes,
                 head * head_size : (head + 1) * head_size,
             ] = mixed[head * nodes : (head + 1) * nodes, :]
     att_sends = []
-    for step in range(ring - 1):
+    for step in reversed(range(ring - 1)):
         copy = pltpu.make_async_remote_copy(
-            att_buf.at[me],
-            att_buf.at[me],
+            att_buf.at[core, me],
+            att_buf.at[core, me],
             att_send_sem.at[step],
-            att_recv_sem.at[me],
-            device_id={"kv": target(step)},
+            att_recv_sem.at[core, me],
+            device_id={"kv": target(step), "tp": last},
         )
         copy.start()
         att_sends.append(copy)
-
-    loads["output_weight"].wait()
-    theirs = pl.ds(pl.multiple_of(partner * half_cols, LANES), half_cols)
-    ours = pl.ds(pl.multiple_of(core * half_cols, LANES), half_cols)
-    output_weight_buf = held["output_weight"]
-    half_sends = []
-    for spot in range(ring):
-        origin = me if spot == 0 else target(ring - 1 - spot)
-        if spot > 0:
-            pltpu.make_async_remote_copy(
-                att_buf.at[origin],
-                att_buf.at[origin],
-                att_send_sem.at[spot - 1],
-                att_recv_sem.at[origin],
-                device_id={"kv": origin},
-            ).wait_recv()
-        attended = att_buf[origin]
-        half_send[spot] = plain_dot(attended, output_weight_buf[:, theirs]).astype(jnp.bfloat16)
-        copy = pltpu.make_async_remote_copy(
+    local_send = pltpu.make_async_remote_copy(
+        att_buf.at[0, me],
+        att_buf.at[0, me],
+        local_send_sem,
+        att_recv_sem.at[0, me],
+        device_id={"tp": last},
+    )
+    pl.when(core != last)(local_send.start)
+
+    origins = [me] + [target(step) for step in range(ring - 1)]
+    half_sends = [
+        pltpu.make_async_remote_copy(
             half_send.at[spot],
             half_recv.at[spot],
             half_send_sem.at[spot],
             half_recv_sem.at[spot],
             device_id={"tp": partner},
         )
-        copy.start()
-        half_sends.append(copy)
-        half_mine[spot] = plain_dot(attended, output_weight_buf[:, ours]).astype(jnp.bfloat16)
-    for spot in range(ring):
-        origin = me if spot == 0 else target(ring - 1 - spot)
-        half_sends[spot].wait_recv()
-        out_ref[origin] = (
-            half_mine[spot].astype(jnp.float32) + half_recv[spot].astype(jnp.float32)
-        ).astype(jnp.bfloat16)
-    for copy in sends + att_sends + half_sends:
+        for spot in range(ring)
+    ]
+
+    @pl.when(core == last)
+    def _():
+        weight_push.wait_recv()
+        for spot, origin in enumerate(origins):
+            for other in range(pair):
+                if spot == 0 and other == last:
+                    continue
+                pltpu.make_async_remote_copy(
+                    att_buf.at[other, origin],
+                    att_buf.at[other, origin],
+                    local_send_sem,
+                    att_recv_sem.at[other, origin],
+                    device_id={"tp": partner},
+                ).wait_recv()
+            for half in range(pair):
+                columns = slice(half * half_cols, (half + 1) * half_cols)
+                total = None
+                for other in range(pair):
+                    term = plain_dot(att_buf[other, origin], full_weight[other, :, columns])
+                    term = term.astype(jnp.bfloat16).astype(jnp.float32)
+                    total = term if total is None else total + term
+                if half == last:
+                    out_ref[origin] = total.astype(jnp.bfloat16)
+                else:
+                    half_send[spot] = total.astype(jnp.bfloat16)
+                    half_sends[spot].start()
+
+    @pl.when(core != last)
+    def _():
+        for spot, origin in enumerate(origins):
+            half_sends[spot].wait_recv()
+            out_ref[origin] = half_recv[spot]
+        weight_push.wait_send()
+        local_send.wait_send()
+
+    for copy in sends + att_sends:
         copy.wait_send()
+
+    @pl.when(core == last)
+    def _():
+        for copy in half_sends:
+            copy.wait_send()
 
 
 def fused(
@@ -709,7 +776,7 @@
         "output_weight": output_weight,
     }
     scalars = ("lengths", "accepted", "pend_log")
-    joined_loads = ("query_weight", "key_weight", "value_weight")
+    joined_loads = ("query_weight", "key_weight", "value_weight", "output_weight")
     names = tuple(name for name in arrays if name not in joined_loads) + joined_loads
     order = tuple(arrays)
     held = [
@@ -729,12 +796,10 @@
             pltpu.VMEM((width, query_cols + 2 * head_size), low),
             pltpu.VMEM((rows, width), low),
             pltpu.VMEM((seqs, heads, nodes, head_size), low),
-            pltpu.VMEM((ring - 1, part_rows, head_size), low),
-            pltpu.VMEM((ring, part_rows, head_size), low),
-            pltpu.VMEM((ring - 1, STAT_ROWS, LANES), wide),
-            pltpu.VMEM((ring, STAT_ROWS, LANES), wide),
-            pltpu.VMEM((ring, chunk_rows, query_cols), low),
-            pltpu.VMEM((ring, chunk_rows, half_cols), low),
+            pltpu.VMEM((ring - 1, part_rows + 2 * STAT_ROWS, head_size), low),
+            pltpu.VMEM((ring, part_rows + 2 * STAT_ROWS, head_size), low),
+            pltpu.VMEM((pair, query_cols, pair * half_cols), low),
+            pltpu.VMEM((pair, ring, chunk_rows, query_cols), low),
             pltpu.VMEM((ring, chunk_rows, half_cols), low),
             pltpu.VMEM((ring, chunk_rows, half_cols), low),
             sems((len(names),)),
@@ -742,11 +807,11 @@
             sems((ring - 1,)),
             sems((ring,)),
             sems((ring - 1,)),
-            sems((ring,)),
-            sems((ring - 1,)),
+            sems((pair, ring)),
             sems((ring,)),
             sems((ring,)),
-            sems((ring,)),
+            sems,
+            sems((2,)),
         ],
         compiler_params=pltpu.CompilerParams(
             collective_id=0, has_side_effects=True, vmem_limit_bytes=VMEM_LIMIT
@@ -772,7 +837,7 @@
         and seqs % ring == 0
         and (seqs // ring * heads * nodes) % LANES == 0
         and STAT_ROWS * (ring + 1) <= LANES
-        and seqs // ring * heads * nodes // LANES <= STAT_ROWS
+        and STAT_PARTS * (seqs // ring * heads * nodes // LANES) <= 2 * STAT_ROWS
         and seqs // ring * nodes + seqs * arrays[13].shape[1] == LANES
         and (seqs * nodes) % LANES == 0
         and output_weight.shape[1] % (pair * LANES) == 0

time: 22.1 us -> 21.6 us (0.977)
  Pallas kernels: 21.3 us -> 20.8 us
    pallas_call x1, Pallas kernels: 21.3 us -> 20.8 us  [fused(): pl.pallas_call(functools.partial(fused_kernel, ring, pair, pieces, names,...]
where the time goes in v1:
time: 21.6 us; the launch traced here: 21.5 us
  Pallas kernels  20.8 us (96%)
  local copies, waits for them, and re-layouts  0.66 us (3%)
    pallas_call x1, Pallas kernels, fused(): pl.pallas_call(functools.partial(fused_kernel, ring, pair, pieces, names,...  20.8 us
    unnamed x1, local copies, waits for them, and re-layouts  0.66 us

profile of v1, /device:TPU:0, one launch (start us, length us, event | category | flops | bytes accessed | tf_op | source)
XLA Modules:
  0.0 21.5 jit_solution(11764223643514663693)
XLA Ops:
  0.0 20.8 %shard_map.181 = bf16[4,64,256]{2,1,0:T(8,128)(2,1)S(1)} custom-call(bf16[256,2048]{1,0:T(8,128)(2,1)} %bitcast.14, f32[1,2048]{1,0:T(1,128)} %bitcast.21, f32[1,128]{1,0:T(1,128)} %bitcast.23, s32[16]{0:T(128)} %refs_3_.1, f32[16,4,256]{2,1,0:T(4,128)} %bitcast.17, bf16[16,256,128]{2,1,0:T(8,128)(2,1)} %bitcast.15, bf16[16,256,128]{2,1,0:T(8,128)(2,1)} %bitcast.16, ...), custom_call_target="tpu_custom_call" | custom-call | tf_op jit(solution)/shard_map/pallas_call | solution.py:789
  20.8 0.7 %copy.21 = bf16[16,16,256]{2,1,0:T(8,128)(2,1)} copy(bf16[16,16,256]{2,1,0:T(8,128)(2,1)S(1)} %bitcast.13) | data formatting | bytes 262144
